TPU v7x, 32 devices: a whole 2x2x4 slice. The times are simulated.
32 devices in a mesh: sp: 8 (over z, x), dp: 4 (over y, core).
Axes of the slice: x: 2, y: 2, z: 4, core: 2. Of those that a mesh axis runs over, the one named last changes fastest.
Arguments:
- queries: bfloat16 [4, 1024, 2048], P('dp', 'sp'), may hold values from -9 to 9
- keys: bfloat16 [4, 1024, 512], P('dp', 'sp'), may hold values from -9 to 9
- values: bfloat16 [4, 1024, 512], P('dp', 'sp'), may hold values from -6 to 6
- out_grad: bfloat16 [4, 1024, 2048], P('dp', 'sp'), may hold values from -24 to 24
- layer_in: bfloat16 [4, 1024, 4096], P('dp', 'sp'), may hold values from -0.1875 to 0.1875
- key_weight: bfloat16 [4096, 512], P('dp'), may hold values from -0.09375 to 0.09375
- value_weight: bfloat16 [4096, 512], P('dp'), may hold values from -0.09375 to 0.09375
- query_gain: float32 [128], replicated, may hold values from 0.64 to 6.04
- key_gain: float32 [128], replicated, may hold values from 0.64 to 6.04
Outputs:
- grad_query: bfloat16 [4, 1024, 2048], P('dp', 'sp')
- grad_in: bfloat16 [4, 1024, 4096], P('dp', 'sp')
- grad_key_weight: float32 [4096, 512], P('dp')
- grad_value_weight: float32 [4096, 512], P('dp')
All inputs are finite; a program needn't handle non-finite values.
Results may differ from a plain program's by a relative error of at most 0.018.
The roundings to bfloat16 on the way count: a program that leaves them out, or rounds other values in their place, can miss the bound.
Values may be sent and summed in bfloat16 or wider, within the bound.
A program may use at most 128 MiB of HBM per device.

v0:
```python
from functools import partial
import math

import jax
import jax.numpy as jnp
from jax import lax
from jax.sharding import PartitionSpec as P

HEADS = 16
KV_HEADS = 4
HEAD_DIM = 128
GRID_W = 64


epsilon = 1e-06
rope_base = 10000.0


def norm_rotate(vector, gain_vec, row_index, col_index):
    scaled = (
        vector * lax.rsqrt(jnp.mean(vector * vector, axis=-1, keepdims=True) + epsilon) * gain_vec
    )
    quarter = vector.shape[-1] // 4
    inverse = rope_base ** (-jnp.arange(quarter, dtype=jnp.float32) / quarter)
    pieces = []
    for offset, position in ((0, row_index), (2 * quarter, col_index)):
        angles = position.astype(jnp.float32)[:, None] * inverse[None, :]
        cosine = jnp.cos(angles)
        sine_part = jnp.sin(angles)
        first_half = scaled[:, offset : offset + quarter]
        second_half = scaled[:, offset + quarter : offset + 2 * quarter]
        pieces.append(first_half * cosine - second_half * sine_part)
        pieces.append(first_half * sine_part + second_half * cosine)
    return jnp.concatenate(pieces, axis=1)


def contract_cols(left_side, right_side):
    return lax.dot_general(
        left_side, right_side, (((1,), (1,)), ((), ())), preferred_element_type=jnp.float32
    )


def contract_rows(left_side, right_side):
    return lax.dot_general(
        left_side, right_side, (((0,), (0,)), ((), ())), preferred_element_type=jnp.float32
    )


def head_grads(query_rows, grad_rows, key_rows, value_rows, query_gain, key_gain):
    length = query_rows.shape[0]
    block_rows = math.gcd(length, 512)
    positions = jnp.arange(length, dtype=jnp.int32)
    row_index = positions // GRID_W
    col_index = positions % GRID_W
    q_rot, q_back = jax.vjp(
        partial(norm_rotate, gain_vec=query_gain, row_index=row_index, col_index=col_index),
        query_rows.astype(jnp.float32),
    )
    k_rot, k_back = jax.vjp(
        partial(norm_rotate, gain_vec=key_gain, row_index=row_index, col_index=col_index),
        key_rows.astype(jnp.float32),
    )
    q_bf = q_rot.astype(jnp.bfloat16)
    k_bf = k_rot.astype(jnp.bfloat16)
    score_scale = q_rot.shape[-1] ** (-0.5)

    def one_block(accums, block_index):
        k_acc, v_acc = accums
        row_start = block_index * block_rows
        q_block = lax.dynamic_slice_in_dim(q_bf, row_start, block_rows, 0)
        g_block = lax.dynamic_slice_in_dim(grad_rows, row_start, block_rows, 0)
        scores = contract_cols(q_block, k_bf) * score_scale
        shifted = jnp.exp(scores - jnp.max(scores, axis=1, keepdims=True))
        attn_probs = shifted / jnp.sum(shifted, axis=1, keepdims=True)
        probs_b = attn_probs.astype(jnp.bfloat16)
        attn_out = jnp.dot(probs_b, value_rows, preferred_element_type=jnp.float32)
        row_delta = jnp.sum(g_block.astype(jnp.float32) * attn_out, axis=1, keepdims=True)
        grad_probs = contract_cols(g_block, value_rows)
        grad_scores = (attn_probs * (grad_probs - row_delta)).astype(jnp.bfloat16)
        q_grad = jnp.dot(grad_scores, k_bf, preferred_element_type=jnp.float32) * score_scale
        k_acc = k_acc + contract_rows(grad_scores, q_block) * score_scale
        v_acc = v_acc + contract_rows(probs_b, g_block)
        return ((k_acc, v_acc), q_grad)

    zeros_init = jnp.zeros(query_rows.shape, jnp.float32)
    (k_acc, v_acc), q_grads = lax.scan(
        one_block, (zeros_init, zeros_init), jnp.arange(length // block_rows, dtype=jnp.int32)
    )
    grad_rq = q_grads.reshape(length, query_rows.shape[1])
    grad_q = q_back(grad_rq)[0].astype(jnp.bfloat16)
    grad_k = k_back(k_acc)[0].astype(jnp.bfloat16)
    return (grad_q, grad_k, v_acc.astype(jnp.bfloat16))


def on_device(
    queries, keys, values, out_grad, layer_in, key_weight, value_weight, query_gain, key_gain
):
    seq_count, tokens_here, _ = queries.shape
    model_width = layer_in.shape[2]
    group_size = HEADS // KV_HEADS
    kv_width = KV_HEADS * HEAD_DIM
    query_part = queries.reshape(seq_count, tokens_here, HEADS, HEAD_DIM)
    grad_part = out_grad.reshape(seq_count, tokens_here, HEADS, HEAD_DIM)
    shape_wide = (seq_count, tokens_here, KV_HEADS, group_size, HEAD_DIM)
    key_part = jnp.broadcast_to(
        keys.reshape(seq_count, tokens_here, KV_HEADS, 1, HEAD_DIM), shape_wide
    ).reshape(seq_count, tokens_here, HEADS, HEAD_DIM)
    value_part = jnp.broadcast_to(
        values.reshape(seq_count, tokens_here, KV_HEADS, 1, HEAD_DIM), shape_wide
    ).reshape(seq_count, tokens_here, HEADS, HEAD_DIM)
    bundle = jnp.concatenate([query_part, grad_part, key_part, value_part], axis=3)
    arrived = lax.all_to_all(bundle, "sp", split_axis=2, concat_axis=1, tiled=True)
    arrived_seqs, length, head_count, _ = arrived.shape
    flat_heads = arrived.transpose(0, 2, 1, 3).reshape(
        arrived_seqs * head_count, length, 4 * HEAD_DIM
    )

    def one_item(one_head):
        grad_q, grad_k, grad_v = head_grads(
            one_head[:, :HEAD_DIM],
            one_head[:, HEAD_DIM : 2 * HEAD_DIM],
            one_head[:, 2 * HEAD_DIM : 3 * HEAD_DIM],
            one_head[:, 3 * HEAD_DIM :],
            query_gain,
            key_gain,
        )
        return jnp.concatenate([grad_q, grad_k, grad_v], axis=1)

    all_grads = lax.map(one_item, flat_heads)
    head_out = all_grads.reshape(arrived_seqs, head_count, length, 3 * HEAD_DIM).transpose(
        0, 2, 1, 3
    )
    token_grads = lax.all_to_all(head_out, "sp", split_axis=1, concat_axis=2, tiled=True)
    grad_query = token_grads[:, :, :, :HEAD_DIM].reshape(seq_count, tokens_here, HEADS * HEAD_DIM)

    def grouped(array):
        summed = jnp.sum(
            array.reshape(seq_count * tokens_here, KV_HEADS, group_size, HEAD_DIM).astype(
                jnp.float32
            ),
            axis=2,
        )
        return summed.astype(jnp.bfloat16).reshape(seq_count * tokens_here, kv_width)

    kv_grad = jnp.concatenate(
        [
            grouped(token_grads[:, :, :, HEAD_DIM : 2 * HEAD_DIM]),
            grouped(token_grads[:, :, :, 2 * HEAD_DIM :]),
        ],
        axis=1,
    )
    stacked = jnp.concatenate([key_weight, value_weight], axis=1)
    grad_flat = contract_cols(kv_grad, lax.all_gather(stacked, "dp", axis=0, tiled=True))
    grad_in = grad_flat.astype(jnp.bfloat16).reshape(seq_count, tokens_here, model_width)
    flat_in = layer_in.reshape(seq_count * tokens_here, model_width)
    partial_sum = lax.psum_scatter(
        contract_rows(flat_in, kv_grad).astype(jnp.bfloat16), "dp", scatter_dimension=0, tiled=True
    )
    weight_grad = lax.psum(partial_sum, "sp").astype(jnp.float32)
    return (grad_query, grad_in, weight_grad[:, :kv_width], weight_grad[:, kv_width:])


def solution(mesh):
    in_specs = (
        P("dp", "sp", None),
        P("dp", "sp", None),
        P("dp", "sp", None),
        P("dp", "sp", None),
        P("dp", "sp", None),
        P("dp", None),
        P("dp", None),
        P(),
        P(),
    )
    out_specs = (P("dp", "sp", None), P("dp", "sp", None), P("dp", None), P("dp", None))
    return jax.shard_map(
        on_device, mesh=mesh, in_specs=in_specs, out_specs=out_specs, check_vma=False
    )
```

profile of v0, /device:TPU:0, one launch (start us, length us, event | category | flops | bytes accessed | tf_op | source)
XLA Modules:
  0.0 448.0 jit_solution(12907583575697410862)
XLA Ops:
  10.6 1.3 copy.112
  12.2 1.5 maximum_bitcast_fusion.1
  13.7 7.3 %all-to-all-start = ((bf16[1,128,16,512]{1,3,0,2:T(8,128)(2,1)}), bf16[1,128,16,512]{1,3,0,2:T(8,128)(2,1)S(1)}, u32[]{:S(2)}, u32[]{:S(2)}) async-start(bf16[1,128,16,512]{1,3,0,2:T(8,128)(2,1)} %maximum_bitcast_fusion.1), calls=%async_computation | async-start | bytes 4194304 | tf_op jit(solution)/shard_map/all_to_all | solution.py:112
  21.0 48.2 %all-to-all-done = bf16[1,128,16,512]{1,3,0,2:T(8,128)(2,1)S(1)} async-done(((bf16[1,128,16,512]{1,3,0,2:T(8,128)(2,1)}), bf16[1,128,16,512]{1,3,0,2:T(8,128)(2,1)S(1)}, u32[]{:S(2)}, u32[]{:S(2)}) %all-to-all-start) | async-done | bytes 2097184 | tf_op jit(solution)/shard_map/all_to_all | solution.py:112
  69.2 2.6 copy.116
  71.8 3.1 copy.117
  74.9 69.9 %while.43 = (s32[]{:T(128)}, bf16[2,1024,384]{1,2,0:T(8,128)(2,1)}, bf16[2,1024,512]{2,1,0:T(8,128)(2,1)}, f32[128]{0:T(128)}, f32[128]{0:T(128)}, /*index=5*/s3...) while((s32[]{:T(128)}, bf16[2,1024,384]{1,2,0:T(8,128)(2,1)}, ...), condition=%wide.region_10.11_spmd, body=%wide.region_0.10_spmd.sunk | while | flops 825649728 | bytes 72149696 | solution.py:129
  74.9 2.3 constant_dynamic-slice_fusion.2
  77.2 1.5 copy.146
  84.2 12.8 %while.44 = (s32[]{:T(128)}, f32[1024,128]{1,0:T(8,128)S(1)}, f32[1024,128]{1,0:T(8,128)S(1)}, f32[2,512,128]{2,1,0:T(8,128)}, s32[2]{0:T(128)S(1)}, /*index=5*/...) while((s32[]{:T(128)}, f32[1024,128]{1,0:T(8,128)S(1)}, ...), condition=%wide.region_7.7_spmd.clone, body=%wide.region_3.6_spmd.clone.sunk | while | flops 813038080 | bytes 26097944 | solution.py:86
  98.0 1.6 fusion.145
  99.7 2.0 copy.151
  101.7 1.9 copy.153
  104.4 2.1 fusion.146
  109.9 2.3 constant_dynamic-slice_fusion.2
  112.2 1.5 copy.146
  119.1 12.8 %while.44 = (s32[]{:T(128)}, f32[1024,128]{1,0:T(8,128)S(1)}, f32[1024,128]{1,0:T(8,128)S(1)}, f32[2,512,128]{2,1,0:T(8,128)}, s32[2]{0:T(128)S(1)}, /*index=5*/...) while((s32[]{:T(128)}, f32[1024,128]{1,0:T(8,128)S(1)}, ...), condition=%wide.region_7.7_spmd.clone, body=%wide.region_3.6_spmd.clone.sunk | while | flops 813038080 | bytes 26097944 | solution.py:86
  132.9 1.6 fusion.145
  134.7 2.0 copy.151
  136.7 1.9 copy.153
  139.4 2.1 fusion.146
  144.8 4.3 copy.119
  149.1 40.6 %all_to_all.36 = bf16[1,1024,2,384]{3,2,0,1:T(2,128)(2,1)S(1)} all-to-all(bf16[1,1024,2,384]{3,2,0,1:T(2,128)(2,1)S(1)} %bitcast.84), channel_id=1, replica_groups=mesh['sp'=8,'dp'=4] {'sp'}, dimensions={1} | all-to-all | bytes 3145728 | tf_op jit(solution)/shard_map/all_to_all | solution.py:133
  191.0 5.5 %convert_bitcast_fusion = bf16[4096,1024]{0,1:T(8,128)(2,1)} fusion(bf16[1,128,4096]{2,1,0:T(8,128)(2,1)S(1)} %copy-done, bf16[128,512]{0,1:T(8,128)(2,1)S(1)} %bitcast.95, bf16[128,512]{0,1:T(8,128)(2,1)S(1)} %bitcast.93), kind=kOutput, calls=%fused_computation.129 | convolution fusion | flops 1078460416 | bytes 9699328 | tf_op jit(solution)/shard_map/dot_general | solution.py:44
  197.8 2.9 pad_maximum_fusion.2
  200.7 66.4 %reduce-scatter.2.cloned.1.call-done = bf16[1024,1024]{0,1:T(8,128)(2,1)} async-done(((bf16[4096,1024]{0,1:T(8,128)(2,1)}), bf16[1024,1024]{0,1:T(8,128)(2,1)}) %reduce-scatter.2.cloned.1.call-update) | async-done | bytes 2097168 | tf_op jit(solution)/shard_map/reduce_scatter | solution.py:156
  268.4 59.1 %all-gather.2.cloned.1.call-done = bf16[4096,1024]{1,0:T(8,128)(2,1)} async-done(((bf16[1024,1024]{1,0:T(8,128)(2,1)}), bf16[4096,1024]{1,0:T(8,128)(2,1)}) %all-gather.2.cloned.1.call-update) | async-done | bytes 8388624 | tf_op jit(solution)/shard_map/all_gather | solution.py:153
  327.5 7.2 %fusion.93 = bf16[1,128,4096]{2,1,0:T(8,128)(2,1)} fusion(bf16[4096,1024]{1,0:T(8,128)(2,1)} %all-gather.2.cloned.1.call-done, bf16[128,512]{0,1:T(8,128)(2,1)S(1)} %bitcast.96, bf16[128,512]{0,1:T(8,128)(2,1)S(1)} %bitcast.94), kind=kOutput, calls=%fused_computation.131 | convolution fusion | flops 1074790400 | bytes 9699328 | tf_op jit(solution)/shard_map/dot_general | solution.py:38
  334.8 98.7 %all-reduce.10.cloned.1.call-done = bf16[1024,1024]{0,1:T(8,128)(2,1)} async-done(((bf16[1024,1024]{0,1:T(8,128)(2,1)}), bf16[1024,1024]{0,1:T(8,128)(2,1)}) %all-reduce.10.cloned.1.call-update) | async-done | bytes 2097168 | tf_op jit(solution)/shard_map/psum | solution.py:159
  433.5 3.3 fusion.99
  436.8 2.9 copy.127
  439.7 1.8 copy.126
  (171 shorter events, 51.4 us)
Async XLA Ops:
  7.2 183.9 %copy-start = (bf16[1,128,4096]{2,1,0:T(8,128)(2,1)S(1)}, bf16[1,128,4096]{2,1,0:T(8,128)(2,1)}, u32[]{:S(2)}) copy-start(bf16[1,128,4096]{2,1,0:T(8,128)(2,1)} %param.17) | copy-start | bytes 3145732
  13.7 55.5 %all-to-all-start = ((bf16[1,128,16,512]{1,3,0,2:T(8,128)(2,1)}), bf16[1,128,16,512]{1,3,0,2:T(8,128)(2,1)S(1)}, u32[]{:S(2)}, u32[]{:S(2)}) async-start(bf16[1,128,16,512]{1,3,0,2:T(8,128)(2,1)} %maximum_bitcast_fusion.1), calls=%async_computation | async-start | bytes 4194304 | tf_op jit(solution)/shard_map/all_to_all | solution.py:112
  21.0 246.2 %reduce-scatter.2.cloned.1.call-start = ((), (), s32[]{:S(2)}) async-start(), calls=%async_computation.4 | async-start | bytes 10485760 | tf_op jit(solution)/shard_map/reduce_scatter | solution.py:156
  74.9 7.8 %copy-start.14 = (f32[32]{0:T(128)}, f32[32]{0:T(128)S(1)}, u32[]{:S(2)}) copy-start(f32[32]{0:T(128)S(1)} %multiply_power_fusion.2) | copy-start | bytes 388 | tf_op jit(solution)/shard_map/while
  78.7 1.6 copy-start.1
  78.8 5.1 %copy-start.12 = (f32[1024]{0:T(1024)}, f32[1024]{0:T(1024)S(1)}, u32[]{:S(2)}) copy-start(f32[1024]{0:T(1024)S(1)} %get-tuple-element.490) | copy-start | bytes 12292 | tf_op jit(solution)/shard_map/while
  88.1 1.1 copy-start.3
  89.7 0.8 copy-start.4
  94.5 1.2 copy-start.3
  96.1 0.8 copy-start.4
  96.9 1.0 copy-start.5
  99.6 4.0 copy-start.6
  99.7 6.8 %copy-start.2 = (bf16[1,1024,512]{1,2,0:T(8,128)(2,1)S(1)}, bf16[1,1024,512]{1,2,0:T(8,128)(2,1)}, u32[]{:S(2)}) copy-start(bf16[1,1024,512]{1,2,0:T(8,128)(2,1)} %copy-done.1) | copy-start | bytes 3145732 | tf_op jit(solution)/shard_map/while
  104.4 3.2 copy-start.11
  104.4 3.2 copy-start.13
  106.6 2.0 copy-start.7
  108.7 1.1 copy-start.8
  109.8 7.8 %copy-start.14 = (f32[32]{0:T(128)}, f32[32]{0:T(128)S(1)}, u32[]{:S(2)}) copy-start(f32[32]{0:T(128)S(1)} %multiply_power_fusion.2) | copy-start | bytes 388 | tf_op jit(solution)/shard_map/while
  113.7 1.6 copy-start.1
  113.8 5.1 %copy-start.12 = (f32[1024]{0:T(1024)}, f32[1024]{0:T(1024)S(1)}, u32[]{:S(2)}) copy-start(f32[1024]{0:T(1024)S(1)} %get-tuple-element.490) | copy-start | bytes 12292 | tf_op jit(solution)/shard_map/while
  123.1 1.2 copy-start.3
  129.5 1.2 copy-start.3
  131.9 1.0 copy-start.5
  134.5 4.0 copy-start.6
  134.7 6.8 %copy-start.2 = (bf16[1,1024,512]{1,2,0:T(8,128)(2,1)S(1)}, bf16[1,1024,512]{1,2,0:T(8,128)(2,1)}, u32[]{:S(2)}) copy-start(bf16[1,1024,512]{1,2,0:T(8,128)(2,1)} %copy-done.1) | copy-start | bytes 3145732 | tf_op jit(solution)/shard_map/while
  139.4 3.2 copy-start.11
  139.4 3.2 copy-start.13
  141.5 2.0 copy-start.7
  143.6 1.1 copy-start.8
  196.6 1.2 copy-start.9
  196.6 130.9 %all-gather.2.cloned.1.call-start = ((), (), s32[]{:S(2)}) async-start(), calls=%async_computation.3 | async-start | bytes 10485760 | tf_op jit(solution)/shard_map/all_gather | solution.py:153
  200.7 232.8 %all-reduce.10.cloned.1.call-start = ((), (), s32[]{:S(2)}) async-start(), calls=%async_computation.5 | async-start | bytes 4194304 | tf_op jit(solution)/shard_map/psum | solution.py:159
  (4 other events, 3.1 us)
Sparse Core Ops, SparseCore 0:
  196.7 70.3 reduce-scatter.1
  269.3 58.2 all-gather.1
  331.2 102.2 all-reduce.9
where the time goes:
time: 449 us; the launch traced here: 448 us
  waiting for transfers between devices  272 us (61%)
  local copies, waits for them, and re-layouts  62.2 us (14%)
  blocking collectives  40.6 us (9%)
  matrix products  26 us (6%)
  other arithmetic  22.1 us (5%)
  between operations  13.9 us (3%)
  starting transfers between devices  7.4 us (2%)
    psum x1, waiting for transfers between devices, on_device(): weight_grad = lax.psum(partial_sum, 'sp').astype(jnp.float32)  98.7 us
    reduce_scatter x1, waiting for transfers between devices, on_device(): lax.psum_scatter(contract_rows(flat_in, kv_grad).astype(jnp.bfloat16), 'd...  66.4 us
    all_gather x1, waiting for transfers between devices, on_device(): lax.all_gather(stacked, 'dp', axis=0, tiled=True)  59.1 us
    all_to_all x1, waiting for transfers between devices, on_device(): lax.all_to_all(bundle, 'sp', split_axis=2, concat_axis=1, tiled=True)  48.2 us
    all_to_all x1, blocking collectives, on_device(): lax.all_to_all(head_out, 'sp', split_axis=1, concat_axis=2, tiled=True)  40.6 us
    while x72, local copies, waits for them, and re-layouts  20.6 us
    dot_general x9, matrix products, contract_cols(): lax.dot_general(left_side, right_side, (((1,), (1,)), ((), ())), preferre...  11.5 us
    dot_general x9, matrix products, contract_rows(): lax.dot_general(left_side, right_side, (((0,), (0,)), ((), ())), preferre...  10.7 us
  transfers between devices with their start and end apart: 4, of which 4 were waited for; matrix products, arithmetic and copies ran while one was open for 3% of the time, Pallas kernels for 0%

commit v1 on v0

v1 whole, which is shorter than its diff:
```python
import functools

import numpy as np
import jax
import jax.numpy as jnp
from jax import lax
from jax.experimental import pallas as pl
from jax.experimental.pallas import tpu as pltpu
from jax.sharding import PartitionSpec as P

HEAD_DIM = 128
GRID_W = 64
EPS = 1e-06
BASE = 10000.0
F32 = jnp.float32
BF16 = jnp.bfloat16


def dot(a, b, ca, cb):
    return lax.dot_general(a, b, (((ca,), (cb,)), ((), ())), preferred_element_type=F32)


def swapped(n):
    lane = lax.broadcasted_iota(jnp.int32, n.shape, 1)
    quarter = HEAD_DIM // 4
    return jnp.where(
        lane % (2 * quarter) < quarter,
        pltpu.roll(n, HEAD_DIM - quarter, 1),
        pltpu.roll(n, quarter, 1),
    )


def norm_rotate(u, gain, cosine, sine):
    r = lax.rsqrt(jnp.mean(u * u, axis=1, keepdims=True) + EPS)
    n = u * r * gain
    return n * cosine + swapped(n) * sine


def norm_rotate_back(u, gain, cosine, sine, grad):
    r = lax.rsqrt(jnp.mean(u * u, axis=1, keepdims=True) + EPS)
    dn = (grad * cosine - swapped(grad) * sine) * gain
    inner = jnp.mean(u * dn, axis=1, keepdims=True)
    return r * dn - u * (r * r * r * inner)


def tables(first, count):
    quarter = HEAD_DIM // 4
    inverse = (BASE ** (-np.arange(quarter) / quarter)).astype(np.float32)
    by_lane = jnp.asarray(np.tile(inverse, 4))[None, :]
    sign = jnp.asarray(np.tile(np.repeat([-1.0, 1.0], quarter), 2).astype(np.float32))[None, :]
    position = first + lax.broadcasted_iota(jnp.int32, (count, HEAD_DIM), 0)
    lane = lax.broadcasted_iota(jnp.int32, (count, HEAD_DIM), 1)
    where = jnp.where(lane < HEAD_DIM // 2, position // GRID_W, position % GRID_W)
    angle = where.astype(F32) * by_lane
    return jnp.cos(angle), jnp.sin(angle) * sign


def rotate_keys_kernel(kv_heads, k_ref, v_ref, gain_ref, cos_ref, sin_ref, out_ref):
    width = kv_heads * HEAD_DIM
    for h in range(kv_heads):
        cols = slice(h * HEAD_DIM, (h + 1) * HEAD_DIM)
        out_ref[:, cols] = norm_rotate(
            k_ref[:, cols].astype(F32), gain_ref[...], cos_ref[...], sin_ref[...]
        ).astype(BF16)
    out_ref[:, width:] = v_ref[...]


def attention_kernel(
    group, q_ref, g_ref, k_ref, v_ref, gain_ref, cos_ref, sin_ref, dq_ref, dkv_ref,
    rq, gs, pb, ds,
):
    rows = q_ref.shape[0]
    scale = HEAD_DIM ** (-0.5)
    k = k_ref[...]
    v = v_ref[...]
    for h in range(group):
        cols = slice(h * HEAD_DIM, (h + 1) * HEAD_DIM)
        here = slice(h * rows, (h + 1) * rows)
        rot = norm_rotate(
            q_ref[:, cols].astype(F32), gain_ref[...], cos_ref[...], sin_ref[...]
        ).astype(BF16)
        grad = g_ref[:, cols]
        rq[here, :] = rot
        gs[here, :] = grad
        scores = dot(rot, k, 1, 1) * scale
        e = jnp.exp(scores - jnp.max(scores, axis=1, keepdims=True))
        probs = e * (1.0 / jnp.sum(e, axis=1, keepdims=True))
        probs_b = probs.astype(BF16)
        out = dot(probs_b, v, 1, 0)
        delta = jnp.sum(grad.astype(F32) * out, axis=1, keepdims=True)
        gp = dot(grad, v, 1, 1)
        pb[here, :] = probs_b
        ds[here, :] = (probs * (gp - delta)).astype(BF16)
    dq = dot(ds[...], k, 1, 0) * scale
    for h in range(group):
        cols = slice(h * HEAD_DIM, (h + 1) * HEAD_DIM)
        dq_ref[:, cols] = norm_rotate_back(
            q_ref[:, cols].astype(F32), gain_ref[...], cos_ref[...], sin_ref[...],
            dq[h * rows : (h + 1) * rows, :],
        ).astype(BF16)
    dk = (dot(rq[...], ds[...], 0, 0) * scale).T.astype(BF16)
    dv = dot(gs[...], pb[...], 0, 0).T.astype(BF16)
    for s in range(dkv_ref.shape[0]):
        dkv_ref[s, 0] = dk[s * rows : (s + 1) * rows, :]
        dkv_ref[s, 1] = dv[s * rows : (s + 1) * rows, :]


def keys_back_kernel(kv_heads, k_ref, d_ref, gain_ref, cos_ref, sin_ref, out_ref):
    width = kv_heads * HEAD_DIM
    for h in range(kv_heads):
        cols = slice(h * HEAD_DIM, (h + 1) * HEAD_DIM)
        out_ref[:, cols] = norm_rotate_back(
            k_ref[:, cols].astype(F32), gain_ref[...], cos_ref[...], sin_ref[...],
            d_ref[0, :, cols].astype(F32),
        ).astype(BF16)
    out_ref[:, width:] = d_ref[1]


def on_device(
    n_sp, n_dp, queries, keys, values, out_grad, layer_in, key_weight, value_weight,
    query_gain, key_gain,
):
    _, rows, q_width = queries.shape
    kv_width = keys.shape[2]
    kv_heads = kv_width // HEAD_DIM
    group = q_width // kv_width
    length = rows * n_sp
    model = layer_in.shape[2]
    q_gain = query_gain[None, :]
    k_gain = key_gain[None, :]
    cosine, sine = tables(lax.axis_index("sp") * rows, rows)

    local = pl.pallas_call(
        functools.partial(rotate_keys_kernel, kv_heads),
        out_shape=jax.ShapeDtypeStruct((rows, 2 * kv_width), BF16),
    )(keys[0], values[0], k_gain, cosine, sine)
    gathered = lax.all_gather(local, "sp", axis=0, tiled=True)
    layer_cols = lax.all_to_all(
        layer_in.reshape(rows, n_dp, model // n_dp), "dp", split_axis=1, concat_axis=0, tiled=True
    ).reshape(n_dp * rows, model // n_dp)

    whole = lambda shape: pl.BlockSpec(shape, lambda i: (0,) * len(shape))
    wide = pl.BlockSpec((rows, group * HEAD_DIM), lambda i: (0, i))
    grad_query, partial = pl.pallas_call(
        functools.partial(attention_kernel, group),
        grid=(kv_heads,),
        in_specs=[
            wide,
            wide,
            pl.BlockSpec((length, HEAD_DIM), lambda i: (0, i)),
            pl.BlockSpec((length, HEAD_DIM), lambda i: (0, i + kv_heads)),
            whole((1, HEAD_DIM)),
            whole((rows, HEAD_DIM)),
            whole((rows, HEAD_DIM)),
        ],
        out_specs=[
            wide,
            pl.BlockSpec((n_sp, 2, rows, HEAD_DIM), lambda i: (0, 0, 0, i)),
        ],
        out_shape=[
            jax.ShapeDtypeStruct((rows, q_width), BF16),
            jax.ShapeDtypeStruct((n_sp, 2, rows, kv_width), BF16),
        ],
        scratch_shapes=[
            pltpu.VMEM((group * rows, HEAD_DIM), BF16),
            pltpu.VMEM((group * rows, HEAD_DIM), BF16),
            pltpu.VMEM((group * rows, length), BF16),
            pltpu.VMEM((group * rows, length), BF16),
        ],
        compiler_params=pltpu.CompilerParams(vmem_limit_bytes=48 * 2**20),
    )(queries[0], out_grad[0], gathered, gathered, q_gain, cosine, sine)

    summed = lax.psum_scatter(partial, "sp", scatter_dimension=0, tiled=True)
    kv_grad = pl.pallas_call(
        functools.partial(keys_back_kernel, kv_heads),
        out_shape=jax.ShapeDtypeStruct((rows, 2 * kv_width), BF16),
    )(keys[0], summed[0], k_gain, cosine, sine)

    kv_all = lax.all_gather(kv_grad, "dp", axis=0, tiled=True)
    part_in = (
        dot(kv_all[:, :kv_width], key_weight, 1, 1) + dot(kv_all[:, kv_width:], value_weight, 1, 1)
    ).astype(BF16)
    grad_in = lax.all_to_all(
        part_in.reshape(n_dp, rows, model // n_dp), "dp", split_axis=0, concat_axis=2, tiled=True
    )
    weight_grad = lax.psum(dot(layer_cols, kv_all, 0, 0).astype(BF16), "sp").astype(F32)
    return (
        grad_query[None],
        grad_in,
        weight_grad[:, :kv_width],
        weight_grad[:, kv_width:],
    )


def solution(mesh):
    tokens = P("dp", "sp", None)
    return jax.shard_map(
        functools.partial(on_device, mesh.shape["sp"], mesh.shape["dp"]),
        mesh=mesh,
        in_specs=(tokens,) * 5 + (P("dp", None), P("dp", None), P(), P()),
        out_specs=(tokens, tokens, P("dp", None), P("dp", None)),
        check_vma=False,
    )
```

time: 449 us -> 298 us (0.66)
  waiting for transfers between devices: 272 us -> 198 us
  local copies, waits for them, and re-layouts: 62.2 us -> 17.9 us
  Pallas kernels: 0 us -> 20.9 us
  matrix products: 26 us -> 5.34 us
  other arithmetic: 22.1 us -> 1.77 us
  starting transfers between devices: 7.4 us -> 0.16 us
    all_to_all x1 -> x0, waiting for transfers between devices: 48.2 us -> none  [on_device(): lax.all_to_all(bundle, 'sp', split_axis=2, concat_axis=1, tiled=True)]
    while x77 -> x0, local copies, waits for them, and re-layouts: 25.5 us -> none
    pallas_call x0 -> x3, Pallas kernels: none -> 20.9 us  [the longest x1 16.4 us: on_device(): pl.pallas_call(functools.partial(attention_kernel, group), grid=(kv_heads...]
    dot_general x26 -> x3, matrix products: 26 us -> 5.34 us  [dot(): lax.dot_general(a, b, (((ca,), (cb,)), ((), ())), preferred_element_type=...]
    psum x1, waiting for transfers between devices: 98.7 us -> 79.5 us  [on_device(): lax.psum(dot(layer_cols, kv_all, 0, 0).astype(BF16), 'sp').astype(F32)]
    dynamic_slice x8 -> x0, local copies, waits for them, and re-layouts: 9.84 us -> none  [the longest x4 7.5 us: on_device(): all_grads = lax.map(one_item, flat_heads)]
    all_to_all x1 -> x0, starting transfers between devices: 7.28 us -> none  [on_device(): lax.all_to_all(bundle, 'sp', split_axis=2, concat_axis=1, tiled=True)]
    all_gather x1 -> x2, waiting for transfers between devices: 59.1 us -> 51.9 us  [the longest x1 51.9 us: on_device(): gathered = lax.all_gather(local, 'sp', axis=0, tiled=True)]
  transfers between devices with their start and end apart: 4 -> 4, of which waited for: 4 -> 3; matrix products, arithmetic and copies ran while one was open for 3% -> 1% of each run, Pallas kernels for 0% -> 0%
where the time goes in v1:
time: 298 us
  waiting for transfers between devices  198 us (66%)
  blocking collectives  39.5 us (13%)
  Pallas kernels  20.9 us (7%)
  local copies, waits for them, and re-layouts  17.9 us (6%)
  between operations  13.9 us (5%)
  matrix products  5.34 us (2%)
    psum x1, waiting for transfers between devices, on_device(): lax.psum(dot(layer_cols, kv_all, 0, 0).astype(BF16), 'sp').astype(F32)  79.5 us
    reduce_scatter x1, waiting for transfers between devices, on_device(): summed = lax.psum_scatter(partial, 'sp', scatter_dimension=0, tiled=True)  66.9 us
    all_gather x1, waiting for transfers between devices, on_device(): gathered = lax.all_gather(local, 'sp', axis=0, tiled=True)  51.9 us
    all_to_all x1, blocking collectives, on_device(): lax.all_to_all(layer_in.reshape(rows, n_dp, model // n_dp), 'dp', split_a...  22.6 us
    all_to_all x1, blocking collectives, on_device(): lax.all_to_all(part_in.reshape(n_dp, rows, model // n_dp), 'dp', split_ax...  16.9 us
    pallas_call x1, Pallas kernels, on_device(): pl.pallas_call(functools.partial(attention_kernel, group), grid=(kv_heads...  16.4 us
    unnamed x23, local copies, waits for them, and re-layouts  13 us
  transfers between devices with their start and end apart: 4, of which 3 were waited for; matrix products, arithmetic and copies ran while one was open for 1% of the time, Pallas kernels for 0%

profile of v1, /device:TPU:0, one launch (start us, length us, event | category | flops | bytes accessed | tf_op | source)
XLA Modules:
  0.0 297.7 jit_solution(17487650503000301759)
XLA Ops:
  7.2 0.0 all-gather.3.cloned.1.call-start
  7.3 1.7 sine_multiply_fusion
  9.0 2.2 shard_map.138
  11.2 0.0 all-gather.3.cloned.1.call-update
  11.2 0.0 reduce-scatter.2.cloned.1.call-start
  11.3 51.9 %all-gather.3.cloned.1.call-done.k_ref.v_ref = bf16[1024,1024]{1,0:T(8,128)(2,1)} async-done(((bf16[128,1024]{1,0:T(8,128)(2,1)}), bf16[1024,1024]{1,0:T(8,128)(2,1)}) %all-gather.3.cloned.1.call-update) | async-done | bytes 2097168 | tf_op jit(solution)/shard_map/all_gather | solution.py:137
  63.2 1.6 copy-done.1
  64.8 0.8 copy-done.2
  65.6 0.8 copy-done.3
  66.5 1.0 copy-done.4
  67.5 1.0 copy-done.5
  68.6 0.7 copy-done.6
  69.2 16.4 %shard_map.139 = (bf16[128,2048]{1,0:T(8,128)(2,1)}, bf16[8,2,128,512]{3,2,1,0:T(8,128)(2,1)}) custom-call(bf16[128,2048]{1,0:T(8,128)(2,1)S(1)} %bitcast.25, bf16[128,2048]{1,0:T(8,128)(2,1)S(1)} %bitcast.26, bf16[1024,1024]{1,0:T(8,128)(2,1)S(1)} %copy-done.1, bf16[1024,1024]{1,0:T(8,128)(2,1)S(1)} %copy-done.1, f32[1,128]{1,0:T(1,128)S(1)} %bitcast.27, ...), custom_call_target="tpu_custom_call" | custom-call | tf_op jit(solution)/shard_map/pallas_call | solution.py:144
  85.6 0.0 all-gather.5.cloned.1.call-start
  85.7 66.9 %reduce-scatter.2.cloned.1.call-done = bf16[1,2,128,512]{3,2,1,0:T(8,128)(2,1)} async-done(((bf16[8,2,128,512]{3,2,1,0:T(8,128)(2,1)}), bf16[1,2,128,512]{3,2,1,0:T(8,128)(2,1)}) %reduce-scatter.2.cloned.1.call-update) | async-done | bytes 262160 | tf_op jit(solution)/shard_map/reduce_scatter | solution.py:173
  152.5 2.3 shard_map.140
  154.9 0.0 all-reduce.2.cloned.1.call-start
  154.9 0.7 copy.22
  155.6 22.6 %all_to_all.33 = bf16[128,4,1024]{0,2,1:T(8,128)(2,1)S(1)} all-to-all(bf16[128,4,1024]{0,2,1:T(8,128)(2,1)S(1)} %bitcast.30), channel_id=1, replica_groups=mesh['sp'=8,'dp'=4] {'dp'}, dimensions={1} | all-to-all | bytes 2097152 | tf_op jit(solution)/shard_map/all_to_all | solution.py:138
  178.2 0.5 copy.23
  178.7 0.0 all-gather.5.cloned.1.call-done
  178.8 3.8 %convert_bitcast_fusion = bf16[1024,1024]{0,1:T(8,128)(2,1)} fusion(bf16[512,1024]{1,0:T(8,128)(2,1)} %all-gather.5.cloned.1.call-done, bf16[512,1024]{1,0:T(8,128)(2,1)S(1)} %bitcast.33), kind=kOutput, calls=%fused_computation | convolution fusion | flops 1074790400 | bytes 4194304 | tf_op jit(solution)/shard_map/dot_general | solution.py:20
  182.6 1.2 copy-done.7
  183.8 0.7 fusion.1
  184.6 0.5 copy-done.9
  185.0 0.8 add_convert_fusion
  185.8 16.9 %all_to_all.34 = bf16[4,128,1024]{2,1,0:T(8,128)(2,1)S(1)} all-to-all(bf16[4,128,1024]{2,1,0:T(8,128)(2,1)S(1)} %bitcast.31), channel_id=1, replica_groups=mesh['sp'=8,'dp'=4] {'dp'}, dimensions={0} | all-to-all | bytes 2097152 | tf_op jit(solution)/shard_map/all_to_all | solution.py:183
  202.7 1.1 copy.26
  203.7 79.5 %all-reduce.2.cloned.1.call-done = bf16[1024,1024]{0,1:T(8,128)(2,1)} async-done(((bf16[1024,1024]{0,1:T(8,128)(2,1)}), bf16[1024,1024]{0,1:T(8,128)(2,1)}) %all-reduce.2.cloned.1.call-update) | async-done | bytes 2097168 | tf_op jit(solution)/shard_map/psum | solution.py:186
  283.2 3.3 %fusion.4 = (f32[1024,512]{0,1:T(8,128)}, f32[1024,512]{0,1:T(8,128)S(1)}) fusion(bf16[1024,1024]{0,1:T(8,128)(2,1)} %all-reduce.2.cloned.1.call-done), kind=kLoop, calls=%fused_computation.17 | loop fusion | bytes 8388608 | tf_op jit(solution)/shard_map/slice | solution.py:191
  286.5 2.9 copy.25
  289.4 1.8 copy.24
  (19 shorter events, 0.1 us)
Async XLA Ops:
  7.2 175.5 %copy-start = (bf16[1024,512]{1,0:T(8,128)(2,1)S(1)}, bf16[1024,512]{1,0:T(8,128)(2,1)}, u32[]{:S(2)}) copy-start(bf16[1024,512]{1,0:T(8,128)(2,1)} %param.16) | copy-start | bytes 3145732
  7.2 56.0 %all-gather.3.cloned.1.call-start = ((), (), s32[]{:S(2)}) async-start(), calls=%async_computation.3 | async-start | bytes 2359296 | tf_op jit(solution)/shard_map/all_gather | solution.py:137
  11.2 141.3 %reduce-scatter.2.cloned.1.call-start = ((), (), s32[]{:S(2)}) async-start(), calls=%async_computation.4 | async-start | bytes 2359296 | tf_op jit(solution)/shard_map/reduce_scatter | solution.py:173
  63.2 1.6 copy-start.1
  64.8 0.8 copy-start.2
  65.6 0.8 copy-start.3
  66.5 1.0 copy-start.4
  67.5 1.0 copy-start.5
  68.6 0.7 copy-start.6
  85.6 69.3 %copy-start.8 = (bf16[1,128,4096]{2,1,0:T(8,128)(2,1)S(1)}, bf16[1,128,4096]{2,1,0:T(8,128)(2,1)}, u32[]{:S(2)}) copy-start(bf16[1,128,4096]{2,1,0:T(8,128)(2,1)} %param.15) | copy-start | bytes 3145732
  85.6 93.1 %all-gather.5.cloned.1.call-start = ((), (), s32[]{:S(2)}) async-start(), calls=%async_computation.5 | async-start | bytes 1310720 | tf_op jit(solution)/shard_map/all_gather | solution.py:179
  154.9 128.3 %all-reduce.2.cloned.1.call-start = ((), (), s32[]{:S(2)}) async-start(), calls=%async_computation.6 | async-start | bytes 4194304 | tf_op jit(solution)/shard_map/psum | solution.py:186
  182.6 1.2 copy-start.7
  183.8 1.2 copy-start.9
Sparse Core Ops, SparseCore 0:
  11.4 51.7 all-gather.2
  85.7 66.7 reduce-scatter.1
  155.0 21.4 all-gather.4
  182.7 100.4 all-reduce.1

commit v2 on v1

v2 whole, which is shorter than its diff:
```python
import functools
import math

import numpy as np
import jax
import jax.numpy as jnp
from jax import lax
from jax.experimental import pallas as pl
from jax.experimental.pallas import tpu as pltpu
from jax.sharding import PartitionSpec as P

HEAD_DIM = 128
GRID_W = 64
EPS = 1e-06
BASE = 10000.0
F32 = jnp.float32
BF16 = jnp.bfloat16


def dot(a, b, ca, cb):
    return lax.dot_general(a, b, (((ca,), (cb,)), ((), ())), preferred_element_type=F32)


def swapped(n):
    lane = lax.broadcasted_iota(jnp.int32, n.shape, 1)
    quarter = HEAD_DIM // 4
    return jnp.where(
        lane % (2 * quarter) < quarter,
        pltpu.roll(n, HEAD_DIM - quarter, 1),
        pltpu.roll(n, quarter, 1),
    )


def norm_rotate(u, gain, cosine, sine):
    r = lax.rsqrt(jnp.mean(u * u, axis=1, keepdims=True) + EPS)
    n = u * r * gain
    return n * cosine + swapped(n) * sine


def norm_rotate_back(u, gain, cosine, sine, grad):
    r = lax.rsqrt(jnp.mean(u * u, axis=1, keepdims=True) + EPS)
    dn = (grad * cosine - swapped(grad) * sine) * gain
    inner = jnp.mean(u * dn, axis=1, keepdims=True)
    return r * dn - u * (r * r * r * inner)


def tables(first, count):
    quarter = HEAD_DIM // 4
    inverse = (BASE ** (-np.arange(quarter) / quarter)).astype(np.float32)
    by_lane = jnp.asarray(np.tile(inverse, 4))[None, :]
    sign = jnp.asarray(np.tile(np.repeat([-1.0, 1.0], quarter), 2).astype(np.float32))[None, :]
    position = first + lax.broadcasted_iota(jnp.int32, (count, HEAD_DIM), 0)
    lane = lax.broadcasted_iota(jnp.int32, (count, HEAD_DIM), 1)
    where = jnp.where(lane < HEAD_DIM // 2, position // GRID_W, position % GRID_W)
    angle = where.astype(F32) * by_lane
    return jnp.cos(angle), jnp.sin(angle) * sign


def ring_order(n):
    across = 2 ** ((n.bit_length() - 1) // 2)
    down = n // across
    cells = [(z, 0) for z in range(down)]
    for z in reversed(range(down)):
        line = [(z, x) for x in range(1, across)]
        cells += line if (down - 1 - z) % 2 == 0 else line[::-1]
    return [z * across + x for z, x in cells]


def pick(table, index):
    return sum(jnp.where(index == i, jnp.int32(v), 0) for i, v in enumerate(table))


def rows_of(c, d, size):
    half = size // 2
    return pl.ds(pl.multiple_of(c * size + d * half, half), half)


def ring_gather(buf, size, n, pos, sides, send, recv, hook=None):
    copies = []
    for s in range(n - 1):
        for d in range(2):
            c = lax.rem(pos + n - s, n) if d == 0 else lax.rem(pos + s, n)
            if s > 0:
                copies[2 * (s - 1) + d].wait_recv()
            part = buf.at[rows_of(c, d, size)]
            copy = pltpu.make_async_remote_copy(
                part, part, send.at[d, s], recv.at[d, s], device_id={"sp": sides[d]}
            )
            copy.start()
            copies.append(copy)
        if s == 0 and hook is not None:
            hook()
    for d in range(2):
        copies[2 * (n - 2) + d].wait_recv()
    for copy in copies:
        copy.wait_send()


def ring_scatter(own, slots, size, n, pos, sides, send, recv, finish, hook=None):
    copies = []
    half = size // 2
    for s in range(n):
        for d in range(2):
            c = lax.rem(pos + 2 * n - s - 1, n) if d == 0 else lax.rem(pos + s + 1, n)
            source = own.at[rows_of(c, d, size)]
            if s > 0:
                copies[2 * (s - 1) + d].wait_recv()
                slot = slots.at[pl.ds((s - 1) * size + d * half, half)]
                total = slot[...].astype(F32) + source[...].astype(F32)
                if s == n - 1:
                    finish(d, total)
                    continue
                slot[...] = total.astype(BF16)
                source = slot
            copy = pltpu.make_async_remote_copy(
                source, slots.at[pl.ds(s * size + d * half, half)],
                send.at[d, s], recv.at[d, s], device_id={"sp": sides[d]},
            )
            copy.start()
            copies.append(copy)
        if s == 0 and hook is not None:
            hook()
    for copy in copies:
        copy.wait_send()


def fused_kernel(
    n_sp, n_dp, q_ref, k_ref, v_ref, g_ref, layer_ref, wk_ref, wv_ref, qg_ref, kg_ref,
    cos_ref, sin_ref, dq_ref, din_ref, gw_ref,
    kv, part, slots, rq, gs, pb, ds, back, lc, kvall, gin, gwpart, gwslots,
    ag_s, ag_r, rs_s, rs_r, ws_s, ws_r, wa_s, wa_r, lx_s, lx_r, kx_s, kx_r, gx_s, gx_r,
):
    rows, q_width = q_ref.shape
    kv_width = k_ref.shape[1]
    kv_heads = kv_width // HEAD_DIM
    group = q_width // kv_width
    length = rows * n_sp
    wide = wk_ref.shape[0]
    share = wide // n_sp
    scale = HEAD_DIM ** (-0.5)
    me = lax.axis_index("sp")
    mine = lax.axis_index("dp")
    order = ring_order(n_sp)
    place = [order.index(i) for i in range(n_sp)]
    pos = pick(place, me)
    sides = (
        pick([order[(place[i] + 1) % n_sp] for i in range(n_sp)], me),
        pick([order[(place[i] - 1) % n_sp] for i in range(n_sp)], me),
    )
    peers = [lax.rem(mine + j, n_dp) for j in range(1, n_dp)]

    barrier = pltpu.get_barrier_semaphore()
    for side in sides:
        pl.semaphore_signal(barrier, inc=1, device_id={"sp": side})
    for peer in peers:
        pl.semaphore_signal(barrier, inc=1, device_id={"dp": peer})
    pl.semaphore_wait(barrier, 2 + len(peers))

    own_rows = pl.ds(pl.multiple_of(pos * rows, rows), rows)
    for h in range(kv_heads):
        cols = slice(h * HEAD_DIM, (h + 1) * HEAD_DIM)
        kv[own_rows, cols] = norm_rotate(
            k_ref[:, cols].astype(F32), kg_ref[...], cos_ref[...], sin_ref[...]
        ).astype(BF16)
    kv[own_rows, kv_width:] = v_ref[...]

    def dcols(j):
        return pl.ds(pl.multiple_of(j * wide, wide), wide)

    def drows(j):
        return pl.ds(pl.multiple_of(j * rows, rows), rows)

    exchange = []

    def start_exchange():
        for j, peer in enumerate(peers):
            copy = pltpu.make_async_remote_copy(
                layer_ref.at[:, dcols(peer)], lc.at[drows(mine)], lx_s.at[j], lx_r.at[j],
                device_id={"dp": peer},
            )
            copy.start()
            exchange.append(copy)
        lc[drows(mine), :] = layer_ref[:, dcols(mine)]

    ring_gather(kv, rows, n_sp, pos, sides, ag_s, ag_r, start_exchange)

    def one_head(i, carry):
        kcols = pl.ds(pl.multiple_of(i * HEAD_DIM, HEAD_DIM), HEAD_DIM)
        vcols = pl.ds(pl.multiple_of(kv_width + i * HEAD_DIM, HEAD_DIM), HEAD_DIM)
        k = kv[:, kcols]
        v = kv[:, vcols]

        def qcols(h):
            return pl.ds(pl.multiple_of((i * group + h) * HEAD_DIM, HEAD_DIM), HEAD_DIM)

        for h in range(group):
            here = slice(h * rows, (h + 1) * rows)
            rot = norm_rotate(
                q_ref[:, qcols(h)].astype(F32), qg_ref[...], cos_ref[...], sin_ref[...]
            ).astype(BF16)
            grad = g_ref[:, qcols(h)]
            rq[here, :] = rot
            gs[here, :] = grad
            scores = dot(rot, k, 1, 1) * scale
            e = jnp.exp(scores - jnp.max(scores, axis=1, keepdims=True))
            probs = e * (1.0 / jnp.sum(e, axis=1, keepdims=True))
            probs_b = probs.astype(BF16)
            out = dot(probs_b, v, 1, 0)
            delta = jnp.sum(grad.astype(F32) * out, axis=1, keepdims=True)
            gp = dot(grad, v, 1, 1)
            pb[here, :] = probs_b
            ds[here, :] = (probs * (gp - delta)).astype(BF16)
        dq = dot(ds[...], k, 1, 0) * scale
        for h in range(group):
            dq_ref[:, qcols(h)] = norm_rotate_back(
                q_ref[:, qcols(h)].astype(F32), qg_ref[...], cos_ref[...], sin_ref[...],
                dq[h * rows : (h + 1) * rows, :],
            ).astype(BF16)
        part[:, kcols] = (dot(rq[...], ds[...], 0, 0) * scale).T.astype(BF16)
        part[:, vcols] = dot(gs[...], pb[...], 0, 0).T.astype(BF16)
        return carry

    lax.fori_loop(0, kv_heads, one_head, 0)

    def keep_back(d, total):
        back[d * (rows // 2) : (d + 1) * (rows // 2), :] = total

    ring_scatter(part, slots, rows, n_sp, pos, sides, rs_s, rs_r, keep_back)

    for h in range(kv_heads):
        cols = slice(h * HEAD_DIM, (h + 1) * HEAD_DIM)
        kvall[drows(mine), cols] = norm_rotate_back(
            k_ref[:, cols].astype(F32), kg_ref[...], cos_ref[...], sin_ref[...], back[:, cols]
        ).astype(BF16)
    kvall[drows(mine), kv_width:] = back[:, kv_width:].astype(BF16)
    spread = []
    for j, peer in enumerate(peers):
        copy = pltpu.make_async_remote_copy(
            kvall.at[drows(mine)], kvall.at[drows(mine)], kx_s.at[j], kx_r.at[j],
            device_id={"dp": peer},
        )
        copy.start()
        spread.append(copy)
    for copy in exchange:
        copy.wait()
    for copy in spread:
        copy.wait()

    block = math.gcd(wide, HEAD_DIM)

    for b in range(wide // block):
        cols = slice(b * block, (b + 1) * block)
        gwpart[cols, :] = dot(lc[:, cols], kvall[...], 0, 0).astype(BF16)

    returned = []

    def inputs_part(j):
        return (
            dot(kvall[drows(j), :kv_width], wk_ref[...], 1, 1)
            + dot(kvall[drows(j), kv_width:], wv_ref[...], 1, 1)
        ).astype(BF16)

    def send_inputs():
        for j, peer in enumerate(peers):
            gin[j] = inputs_part(peer)
            copy = pltpu.make_async_remote_copy(
                gin.at[j], din_ref.at[:, dcols(mine)], gx_s.at[j], gx_r.at[j],
                device_id={"dp": peer},
            )
            copy.start()
            returned.append(copy)
        din_ref[:, dcols(mine)] = inputs_part(mine)

    def keep_weight(d, total):
        gw_ref[rows_of(pos, d, share), :] = total.astype(BF16)

    ring_scatter(
        gwpart, gwslots, share, n_sp, pos, sides, ws_s, ws_r, keep_weight, send_inputs
    )
    ring_gather(gw_ref, share, n_sp, pos, sides, wa_s, wa_r)
    for copy in returned:
        copy.wait()


def on_device(
    n_sp, n_dp, queries, keys, values, out_grad, layer_in, key_weight, value_weight,
    query_gain, key_gain,
):
    _, rows, q_width = queries.shape
    kv_width = keys.shape[2]
    group = q_width // kv_width
    length = rows * n_sp
    model = layer_in.shape[2]
    wide = model // n_dp
    both = 2 * kv_width
    cosine, sine = tables(lax.axis_index("sp") * rows, rows)
    ring = pltpu.SemaphoreType.DMA((2, n_sp - 1))
    direct = pltpu.SemaphoreType.DMA((n_dp - 1,))
    vmem = pl.BlockSpec(memory_space=pltpu.VMEM)
    grad_query, grad_in, weight_grad = pl.pallas_call(
        functools.partial(fused_kernel, n_sp, n_dp),
        in_specs=[vmem] * 11,
        out_specs=[vmem] * 3,
        out_shape=[
            jax.ShapeDtypeStruct((rows, q_width), BF16),
            jax.ShapeDtypeStruct((rows, model), BF16),
            jax.ShapeDtypeStruct((wide, both), BF16),
        ],
        scratch_shapes=[
            pltpu.VMEM((length, both), BF16),
            pltpu.VMEM((length, both), BF16),
            pltpu.VMEM(((n_sp - 1) * rows, both), BF16),
            pltpu.VMEM((group * rows, HEAD_DIM), BF16),
            pltpu.VMEM((group * rows, HEAD_DIM), BF16),
            pltpu.VMEM((group * rows, length), BF16),
            pltpu.VMEM((group * rows, length), BF16),
            pltpu.VMEM((rows, both), F32),
            pltpu.VMEM((n_dp * rows, wide), BF16),
            pltpu.VMEM((n_dp * rows, both), BF16),
            pltpu.VMEM((n_dp - 1, rows, wide), BF16),
            pltpu.VMEM((wide, both), BF16),
            pltpu.VMEM((wide * (n_sp - 1) // n_sp, both), BF16),
        ] + [ring] * 8 + [direct] * 6,
        compiler_params=pltpu.CompilerParams(
            collective_id=0, has_side_effects=True, vmem_limit_bytes=58 * 2**20
        ),
    )(
        queries[0], keys[0], values[0], out_grad[0], layer_in[0], key_weight, value_weight,
        query_gain[None, :], key_gain[None, :], cosine, sine,
    )
    weight_grad = weight_grad.astype(F32)
    return (
        grad_query[None],
        grad_in[None],
        weight_grad[:, :kv_width],
        weight_grad[:, kv_width:],
    )


def solution(mesh):
    tokens = P("dp", "sp", None)
    return jax.shard_map(
        functools.partial(on_device, mesh.shape["sp"], mesh.shape["dp"]),
        mesh=mesh,
        in_specs=(tokens,) * 5 + (P("dp", None), P("dp", None), P(), P()),
        out_specs=(tokens, tokens, P("dp", None), P("dp", None)),
        check_vma=False,
    )
```

time: 298 us -> 171 us (0.57)
  waiting for transfers between devices: 198 us -> 0 us
  Pallas kernels: 20.9 us -> 162 us
  blocking collectives: 39.5 us -> 0 us
  between operations: 13.9 us -> 0.68 us
  local copies, waits for them, and re-layouts: 17.9 us -> 6.03 us
  matrix products: 5.34 us -> 0 us
    pallas_call x3 -> x1, Pallas kernels: 20.9 us -> 162 us  [on_device(): pl.pallas_call(functools.partial(fused_kernel, n_sp, n_dp), in_specs=[vme...]
    psum x1 -> x0, waiting for transfers between devices: 79.5 us -> none  [on_device(): lax.psum(dot(layer_cols, kv_all, 0, 0).astype(BF16), 'sp').astype(F32)]
    reduce_scatter x1 -> x0, waiting for transfers between devices: 66.9 us -> none  [on_device(): summed = lax.psum_scatter(partial, 'sp', scatter_dimension=0, tiled=True)]
    all_gather x2 -> x0, waiting for transfers between devices: 51.9 us -> none  [the longest x1 51.9 us: on_device(): gathered = lax.all_gather(local, 'sp', axis=0, tiled=True)]
    all_to_all x2 -> x0, blocking collectives: 39.5 us -> none  [the longest x1 22.6 us: on_device(): lax.all_to_all(layer_in.reshape(rows, n_dp, model // n_dp), 'dp', split_a...]
    unnamed x23 -> x6, local copies, waits for them, and re-layouts: 13 us -> 1.77 us
    dot_general x3 -> x0, matrix products: 5.34 us -> none  [dot(): lax.dot_general(a, b, (((ca,), (cb,)), ((), ())), preferred_element_type=...]
  transfers between devices with their start and end apart: 4 -> 0, of which waited for: 3 -> 0; matrix products, arithmetic and copies ran while one was open for 1% -> 0% of each run, Pallas kernels for 0% -> 0%
where the time goes in v2:
time: 171 us; the launch traced here: 170 us
  Pallas kernels  162 us (95%)
  local copies, waits for them, and re-layouts  6.03 us (4%)
  other arithmetic  1.71 us (1%)
    pallas_call x1, Pallas kernels, on_device(): pl.pallas_call(functools.partial(fused_kernel, n_sp, n_dp), in_specs=[vme...  162 us
    slice x1, local copies, waits for them, and re-layouts, on_device(): weight_grad[:, kv_width:]  4.26 us

profile of v2, /device:TPU:0, one launch (start us, length us, event | category | flops | bytes accessed | tf_op | source)
XLA Modules:
  0.0 170.4 jit_solution(16452059768803368181)
XLA Ops:
  0.7 1.7 sine_multiply_fusion
  2.4 162.0 %shard_map.138 = (bf16[128,2048]{1,0:T(8,128)(2,1)}, bf16[128,4096]{1,0:T(8,128)(2,1)}, bf16[1024,1024]{1,0:T(8,128)(2,1)}) custom-call(bf16[128,2048]{1,0:T(8,128)(2,1)} %bitcast.11, bf16[128,512]{1,0:T(8,128)(2,1)} %bitcast.14, bf16[128,512]{1,0:T(8,128)(2,1)} %bitcast.15, bf16[128,2048]{1,0:T(8,128)(2,1)} %bitcast.12, bf16[128,4096]{1,0:T(8,128)(2,1)} %bitcast.9, ...), custom_call_target="tpu_custom_call" | custom-call | tf_op jit(solution)/shard_map/pallas_call | solution.py:300
  164.3 0.0 copy-start.1
  164.3 0.0 copy-start
  164.3 4.3 %fusion.1 = (f32[1024,512]{1,0:T(8,128)}, f32[1024,512]{1,0:T(8,128)}) fusion(bf16[1024,1024]{1,0:T(8,128)(2,1)} %get-tuple-element.9), kind=kLoop, calls=%fused_computation.12 | loop fusion | bytes 8388608 | tf_op jit(solution)/shard_map/slice | solution.py:336
  168.6 0.0 copy-done.1
  168.6 0.8 copy.17
  169.4 0.0 copy-done
  169.4 1.0 copy.18
  (4 shorter events, 0.0 us)
Async XLA Ops:
  164.3 4.3 %copy-start.1 = (bf16[128,2048]{1,0:T(8,128)(2,1)S(1)}, bf16[128,2048]{1,0:T(8,128)(2,1)}, u32[]{:S(2)}) copy-start(bf16[128,2048]{1,0:T(8,128)(2,1)} %get-tuple-element.7) | copy-start | bytes 1572868
  164.3 5.1 %copy-start = (bf16[128,4096]{1,0:T(8,128)(2,1)S(1)}, bf16[128,4096]{1,0:T(8,128)(2,1)}, u32[]{:S(2)}) copy-start(bf16[128,4096]{1,0:T(8,128)(2,1)} %get-tuple-element.8) | copy-start | bytes 3145732

commit v3 on v2

--- a/solution.py
+++ b/solution.py
@@ -13,6 +13,7 @@
 GRID_W = 64
 EPS = 1e-06
 BASE = 10000.0
+PIECES = 4
 F32 = jnp.float32
 BF16 = jnp.bfloat16
 
@@ -75,52 +76,60 @@
     return pl.ds(pl.multiple_of(c * size + d * half, half), half)
 
 
+def lanes_of(ref, q):
+    width = ref.shape[1] // PIECES
+    return pl.ds(q * width, width)
+
+
 def ring_gather(buf, size, n, pos, sides, send, recv, hook=None):
-    copies = []
+    copies = {}
+    streams = [(d, q) for q in range(PIECES) for d in range(2)]
     for s in range(n - 1):
-        for d in range(2):
+        for d, q in streams:
             c = lax.rem(pos + n - s, n) if d == 0 else lax.rem(pos + s, n)
             if s > 0:
-                copies[2 * (s - 1) + d].wait_recv()
-            part = buf.at[rows_of(c, d, size)]
-            copy = pltpu.make_async_remote_copy(
-                part, part, send.at[d, s], recv.at[d, s], device_id={"sp": sides[d]}
+                copies[s - 1, d, q].wait_recv()
+            part = buf.at[rows_of(c, d, size), lanes_of(buf, q)]
+            copies[s, d, q] = pltpu.make_async_remote_copy(
+                part, part, send.at[d * PIECES + q, s], recv.at[d * PIECES + q, s],
+                device_id={"sp": sides[d]},
             )
-            copy.start()
-            copies.append(copy)
+            copies[s, d, q].start()
         if s == 0 and hook is not None:
             hook()
-    for d in range(2):
-        copies[2 * (n - 2) + d].wait_recv()
-    for copy in copies:
+    for d, q in streams:
+        copies[n - 2, d, q].wait_recv()
+    for copy in copies.values():
         copy.wait_send()
 
 
 def ring_scatter(own, slots, size, n, pos, sides, send, recv, finish, hook=None):
-    copies = []
+    copies = {}
     half = size // 2
+    streams = [(d, q) for q in range(PIECES) for d in range(2)]
     for s in range(n):
-        for d in range(2):
+        for d, q in streams:
             c = lax.rem(pos + 2 * n - s - 1, n) if d == 0 else lax.rem(pos + s + 1, n)
-            source = own.at[rows_of(c, d, size)]
+            cols = lanes_of(own, q)
+            source = own.at[rows_of(c, d, size), cols]
             if s > 0:
-                copies[2 * (s - 1) + d].wait_recv()
-                slot = slots.at[pl.ds((s - 1) * size + d * half, half)]
+                copies[s - 1, d, q].wait_recv()
+                slot = slots.at[pl.ds((s - 1) * size + d * half, half), cols]
                 total = slot[...].astype(F32) + source[...].astype(F32)
                 if s == n - 1:
-                    finish(d, total)
+                    finish(d, cols, total)
                     continue
                 slot[...] = total.astype(BF16)
                 source = slot
-            copy = pltpu.make_async_remote_copy(
-                source, slots.at[pl.ds(s * size + d * half, half)],
-                send.at[d, s], recv.at[d, s], device_id={"sp": sides[d]},
+            copies[s, d, q] = pltpu.make_async_remote_copy(
+                source, slots.at[pl.ds(s * size + d * half, half), cols],
+                send.at[d * PIECES + q, s], recv.at[d * PIECES + q, s],
+                device_id={"sp": sides[d]},
             )
-            copy.start()
-            copies.append(copy)
+            copies[s, d, q].start()
         if s == 0 and hook is not None:
             hook()
-    for copy in copies:
+    for copy in copies.values():
         copy.wait_send()
 
 
@@ -222,8 +231,8 @@
 
     lax.fori_loop(0, kv_heads, one_head, 0)
 
-    def keep_back(d, total):
-        back[d * (rows // 2) : (d + 1) * (rows // 2), :] = total
+    def keep_back(d, cols, total):
+        back[d * (rows // 2) : (d + 1) * (rows // 2), cols] = total
 
     ring_scatter(part, slots, rows, n_sp, pos, sides, rs_s, rs_r, keep_back)
 
@@ -271,8 +280,8 @@
             returned.append(copy)
         din_ref[:, dcols(mine)] = inputs_part(mine)
 
-    def keep_weight(d, total):
-        gw_ref[rows_of(pos, d, share), :] = total.astype(BF16)
+    def keep_weight(d, cols, total):
+        gw_ref[rows_of(pos, d, share), cols] = total.astype(BF16)
 
     ring_scatter(
         gwpart, gwslots, share, n_sp, pos, sides, ws_s, ws_r, keep_weight, send_inputs
@@ -294,7 +303,7 @@
     wide = model // n_dp
     both = 2 * kv_width
     cosine, sine = tables(lax.axis_index("sp") * rows, rows)
-    ring = pltpu.SemaphoreType.DMA((2, n_sp - 1))
+    ring = pltpu.SemaphoreType.DMA((2 * PIECES, n_sp - 1))
     direct = pltpu.SemaphoreType.DMA((n_dp - 1,))
     vmem = pl.BlockSpec(memory_space=pltpu.VMEM)
     grad_query, grad_in, weight_grad = pl.pallas_call(

time: 171 us -> 142 us (0.83)
  Pallas kernels: 162 us -> 133 us
    pallas_call x1, Pallas kernels: 162 us -> 133 us  [on_device(): pl.pallas_call(functools.partial(fused_kernel, n_sp, n_dp), in_specs=[vme...]
where the time goes in v3:
time: 142 us
  Pallas kernels  133 us (94%)
  local copies, waits for them, and re-layouts  6.03 us (4%)
  other arithmetic  1.71 us (1%)
    pallas_call x1, Pallas kernels, on_device(): pl.pallas_call(functools.partial(fused_kernel, n_sp, n_dp), in_specs=[vme...  133 us
    slice x1, local copies, waits for them, and re-layouts, on_device(): weight_grad[:, kv_width:]  4.26 us

profile of v3, /device:TPU:0, one launch (start us, length us, event | category | flops | bytes accessed | tf_op | source)
XLA Modules:
  0.0 141.8 jit_solution(58621253721678159)
XLA Ops:
  0.7 1.7 %sine_multiply_fusion = (f32[128,128]{1,0:T(8,128)}, f32[128,128]{1,0:T(8,128)}) fusion(f32[128]{0:T(128)} %constant.46.clone, f32[128]{0:T(128)} %constant.45.clone, s32[128]{0:T(128)S(1)} %get-tuple-element.17, s32[128]{0:T(128)S(1)} %get-tuple-element.19, s32[128]{0:T(128)S(1)} %get-tuple-element.16, s32[128]{0:T(128)S(1)} %get-tuple-element.18, ...), kind=kLoop, calls=%fused_computation | loop fusion | flops 98304 | bytes 134528 | tf_op jit(solution)/shard_map/mul | solution.py:57
  2.4 133.3 %shard_map.138 = (bf16[128,2048]{1,0:T(8,128)(2,1)}, bf16[128,4096]{1,0:T(8,128)(2,1)}, bf16[1024,1024]{1,0:T(8,128)(2,1)}) custom-call(bf16[128,2048]{1,0:T(8,128)(2,1)} %bitcast.11, bf16[128,512]{1,0:T(8,128)(2,1)} %bitcast.14, bf16[128,512]{1,0:T(8,128)(2,1)} %bitcast.15, bf16[128,2048]{1,0:T(8,128)(2,1)} %bitcast.12, bf16[128,4096]{1,0:T(8,128)(2,1)} %bitcast.9, ...), custom_call_target="tpu_custom_call" | custom-call | tf_op jit(solution)/shard_map/pallas_call | solution.py:309
  135.7 0.0 copy-start.1
  135.7 0.0 copy-start
  135.7 4.3 %fusion.1 = (f32[1024,512]{1,0:T(8,128)}, f32[1024,512]{1,0:T(8,128)}) fusion(bf16[1024,1024]{1,0:T(8,128)(2,1)} %get-tuple-element.9), kind=kLoop, calls=%fused_computation.12 | loop fusion | bytes 8388608 | tf_op jit(solution)/shard_map/slice | solution.py:345
  140.0 0.0 copy-done.1
  140.0 0.8 copy.17
  140.8 0.0 copy-done
  140.8 1.0 copy.18
  (4 shorter events, 0.0 us)
Async XLA Ops:
  135.7 4.3 %copy-start.1 = (bf16[128,2048]{1,0:T(8,128)(2,1)S(1)}, bf16[128,2048]{1,0:T(8,128)(2,1)}, u32[]{:S(2)}) copy-start(bf16[128,2048]{1,0:T(8,128)(2,1)} %get-tuple-element.7) | copy-start | bytes 1572868
  135.7 5.1 %copy-start = (bf16[128,4096]{1,0:T(8,128)(2,1)S(1)}, bf16[128,4096]{1,0:T(8,128)(2,1)}, u32[]{:S(2)}) copy-start(bf16[128,4096]{1,0:T(8,128)(2,1)} %get-tuple-element.8) | copy-start | bytes 3145732
